TPU v7x, 128 devices: a whole 4x4x4 slice. The times are simulated.
128 devices in a mesh: sp: 32 (over z, y, core), tp: 4 (over x).
Axes of the slice: x: 4, y: 4, z: 4, core: 2. Of those that a mesh axis runs over, the one named last changes fastest.
Arguments:
- queries: bfloat16 [16384, 1024], P('sp', 'tp'), may hold values from -260 to 260, as said below
- keys: bfloat16 [16384, 512], P('sp', 'tp'), may hold values from -8 to 8, as said below
- values: bfloat16 [16384, 512], P('sp', 'tp'), may hold values from -24 to 24
- doc_ids: int32 [16384], P('sp'), may hold values from 0 to 7, never falling along the last dimension, each value on 1 to 8192 neighbouring positions
- sink_logit: float32 [8], P('tp'), may hold values from 2 to 7
- residual_in: bfloat16 [16384, 2048], P(('sp', 'tp')), may hold values from -6 to 6
- w_out: bfloat16 [1024, 2048], replicated, may hold values from -0.375 to 0.375
- gain_one: float32 [2048], replicated, may hold values from 0.1 to 1.9
- w_gate: bfloat16 [2048, 5632], P('sp', 'tp'), may hold values from -0.125 to 0.125
- w_up: bfloat16 [2048, 5632], P('sp', 'tp'), may hold values from -0.125 to 0.125
- w_down: bfloat16 [5632, 2048], P('tp', 'sp'), may hold values from -0.078125 to 0.078125
- gain_two: float32 [2048], replicated, may hold values from 0.1 to 1.9
Outputs:
- layer_out: bfloat16 [16384, 2048], P(('sp', 'tp'))
Inputs may be any that keep to these rules, and one draw needn't show every extreme that they name: Real-valued projected queries. Real-valued projected keys. `doc_ids`: document numbers never fall along the sequence; each document is one run of positions.
All inputs are finite; a program needn't handle non-finite values.
Results may differ from a plain program's by a relative error of at most 0.012.
Values may be sent and summed in bfloat16 or wider, within the bound.
No kernel may reach another device: no remote copies, remote signals or barrier semaphores. Data moves between devices by JAX's collectives and lax.ppermute only.
A program may use at most 128 MiB of HBM per device.

v0:
```python
import math
import jax
import jax.numpy as jnp
from jax import lax
from jax.sharding import PartitionSpec as P

HEAD = 128
HALF = 128
ALPHA = 2.0**0.5
EPS = 1e-05
NEGATIVE = -1e30


def shifted(value, axis, steps):
    count = lax.axis_size(axis)
    leading, last = (max(0, -steps), min(count, count - steps))
    return lax.ppermute(value, axis, [(source, source + steps) for source in range(leading, last)])


def split_up(value, dim, devices):
    before, after = (value.shape[:dim], value.shape[dim + 1 :])
    return jnp.moveaxis(value.reshape(*before, devices, -1, *after), dim, 0)


def sum_at_owner(value, axis, dim):
    devices = lax.axis_size(axis)
    tiles = lax.all_to_all(split_up(value, dim, devices), axis, 0, 0, tiled=True)
    return jnp.sum(tiles.astype(jnp.float32), axis=0)


def laid_out(tiles, dim):
    lengths = list(tiles.shape[1:])
    lengths[dim] *= tiles.shape[0]
    return jnp.moveaxis(tiles, 0, dim).reshape(lengths)


def sent_to_all(value, axis):
    copies = jnp.broadcast_to(value, (lax.axis_size(axis), *value.shape))
    return lax.all_to_all(copies, axis, split_axis=0, concat_axis=0, tiled=True)


def gather_directly(value, axis, dim):
    return laid_out(sent_to_all(value, axis), dim)


def in_one_piece(arrays, axis, dim, along):
    ends, at = ([], 0)
    for a in arrays[:-1]:
        at += a.shape[along]
        ends.append(at)
    both = jnp.concatenate(arrays, axis=along)
    return tuple(jnp.split(lax.all_gather(both, axis, axis=dim, tiled=True), ends, axis=along))


def layer_norm(values_in, gain):
    average = jnp.mean(values_in, -1, keepdims=True)
    centred = values_in - average
    variance = jnp.mean(centred * centred, -1, keepdims=True)
    return centred * lax.rsqrt(variance + EPS) * gain


def per_device(
    queries,
    keys,
    values,
    doc_ids,
    sink_logit,
    residual_in,
    w_out,
    gain_one,
    w_gate,
    w_up,
    w_down,
    gain_two,
):
    row_count = queries.shape[0]
    sp_size = lax.axis_size("sp")
    kv_local = keys.shape[1] // HEAD
    repeat = queries.shape[1] // keys.shape[1]
    lower = (keys[row_count - HALF :], values[row_count - HALF :], doc_ids[row_count - HALF :])
    upper = (keys[:HALF], values[:HALF], doc_ids[:HALF])
    before = shifted((lower[0], lower[1], lower[2]), "sp", 1)
    after = shifted((upper[0], upper[1], upper[2]), "sp", -1)
    keys_all = jnp.concatenate([before[0], keys, after[0]], 0)
    values_all = jnp.concatenate([before[1], values, after[1]], 0)
    docs_all = jnp.concatenate([before[2], doc_ids, after[2]], 0)
    first_pos = lax.axis_index("sp") * row_count
    block = math.gcd(512, row_count)
    span = block + 2 * HALF
    sinks = sink_logit.reshape(kv_local, repeat)

    def one_block(index):
        start = index * block
        query_blk = queries.reshape(block, kv_local, repeat, HEAD)
        key_blk = keys_all.reshape(span, kv_local, HEAD)
        value_blk = values_all.reshape(span, kv_local, HEAD)
        pos_query = first_pos + start + jnp.arange(block, dtype=jnp.int32)
        pos_key = first_pos + start - HALF + jnp.arange(span, dtype=jnp.int32)
        offset = pos_key[None, :] - pos_query[:, None]
        allowed = (jnp.abs(offset) <= HALF) & (docs_all[None, :] == doc_ids[:, None])
        allowed = allowed & (pos_key[None, :] >= 0) & (pos_key[None, :] < sp_size * row_count)
        scores = jnp.einsum(
            "qgrd,kgd->grqk", query_blk, key_blk, preferred_element_type=jnp.float32
        ) * HEAD ** (-0.5)
        scores = jnp.where(allowed[None, None], scores, NEGATIVE)
        top = jnp.maximum(jnp.max(scores, -1), sinks[:, :, None])
        weights = jnp.exp(scores - top[..., None])
        total = jnp.sum(weights, -1) + jnp.exp(sinks[:, :, None] - top)
        summed = jnp.einsum(
            "grqk,kgd->qgrd",
            weights.astype(jnp.bfloat16),
            value_blk,
            preferred_element_type=jnp.float32,
        )
        scaled = summed / jnp.transpose(total, (2, 0, 1))[..., None]
        return scaled.reshape(block, kv_local * repeat * HEAD).astype(jnp.bfloat16)

    attended = lax.map(one_block, jnp.arange(row_count // block, dtype=jnp.int32)).reshape(
        row_count, -1
    )
    width = attended.shape[1]
    own_rows = lax.dynamic_slice_in_dim(w_out, lax.axis_index("tp") * width, width, 0)
    mixed_rows = sum_at_owner(
        jnp.dot(attended, own_rows, preferred_element_type=jnp.float32).astype(jnp.bfloat16),
        "tp",
        0,
    )
    pre_one = ALPHA * residual_in.astype(jnp.float32) + mixed_rows
    normed = layer_norm(pre_one, gain_one).astype(jnp.bfloat16)
    whole_rows = gather_directly(normed, "tp", 0)
    gate_whole, up_whole = in_one_piece((w_gate, w_up), "sp", 0, 1)
    gate_part = jnp.dot(whole_rows, gate_whole, preferred_element_type=jnp.float32)
    up_part = jnp.dot(whole_rows, up_whole, preferred_element_type=jnp.float32)
    hidden = (jax.nn.silu(gate_part) * up_part).astype(jnp.bfloat16)
    down_terms = jnp.dot(
        hidden, lax.all_gather(w_down, "sp", axis=1, tiled=True), preferred_element_type=jnp.float32
    )
    rounded = lax.optimization_barrier(down_terms.astype(jnp.bfloat16)).astype(jnp.float32)
    down_rows = sum_at_owner(rounded.astype(jnp.bfloat16), "tp", 0)
    pre_two = ALPHA * normed.astype(jnp.float32) + down_rows
    return layer_norm(pre_two, gain_two).astype(jnp.bfloat16)


def solution(mesh):
    in_specs = (
        P("sp", "tp"),
        P("sp", "tp"),
        P("sp", "tp"),
        P("sp"),
        P("tp"),
        P(("sp", "tp"), None),
        P(),
        P(),
        P("sp", "tp"),
        P("sp", "tp"),
        P("tp", "sp"),
        P(),
    )
    out_specs = P(("sp", "tp"), None)
    return jax.shard_map(
        per_device, mesh=mesh, in_specs=in_specs, out_specs=out_specs, check_vma=False
    )
```

profile of v0, /device:TPU:0, one launch (start us, length us, event | category | flops | bytes accessed | tf_op | source)
XLA Modules:
  0.0 175.9 jit_solution(14779466636091817606)
XLA Ops:
  6.5 0.0 copy-start
  6.5 0.0 all-gather.3.cloned.1.call-start
  6.5 1.8 %pad_maximum_fusion = bf16[64,2816]{1,0:T(8,128)(2,1)} fusion(bf16[64,1408]{1,0:T(8,128)(2,1)} %param.21, bf16[64,1408]{1,0:T(8,128)(2,1)} %param.20), kind=kLoop, calls=%fused_computation.32 | loop fusion | flops 720896 | bytes 720896 | tf_op jit(solution)/shard_map/concatenate | solution.py:51
  8.4 0.0 copy-start.4
  8.4 0.0 all-gather.3.cloned.1.call-update
  8.4 0.0 all-gather.5.cloned.1.call-start
  8.4 0.7 all-gather.5.cloned.1.call-update
  9.1 0.8 fusion.59
  9.9 1.3 collective-permute-start.2
  11.2 1.3 collective-permute-start.3
  12.5 0.8 fusion.58
  13.3 4.9 %collective-permute-start.4 = (bf16[128,128]{1,0:T(8,128)(2,1)S(1)}, bf16[128,128]{1,0:T(8,128)(2,1)S(1)}, u32[]{:S(2)}, u32[]{:S(2)}) collective-permute-start(bf16[128,128]{1,0:T(8,128)(2,1)S(1)} %get-tuple-element.23), channel_id=1, source_target_pairs={{0,4},{4,8},{8,12},{12,16},{16,20},{20,24},{24,28},{28,32},{32,36}... | collective-permute-start | bytes 98312 | tf_op jit(solution)/shard_map/ppermute | solution.py:17
  18.2 1.3 collective-permute-start.5
  19.5 1.0 copy.13
  20.5 4.3 %collective-permute-start = (bf16[128,128]{0,1:T(8,128)(2,1)S(1)}, bf16[128,128]{0,1:T(8,128)(2,1)S(1)}, u32[]{:S(2)}, u32[]{:S(2)}) collective-permute-start(bf16[128,128]{0,1:T(8,128)(2,1)S(1)} %get-tuple-element.21), channel_id=1, source_target_pairs={{0,4},{4,8},{8,12},{12,16},{16,20},{20,24},{24,28},{28,32},{32,36}... | collective-permute-start | bytes 98312 | tf_op jit(solution)/shard_map/ppermute | solution.py:17
  24.9 0.0 collective-permute-done.2
  24.9 1.3 collective-permute-start.1
  26.2 0.0 collective-permute-done.3
  26.2 0.7 pad_add_fusion
  26.9 1.6 fusion.18
  28.5 0.0 collective-permute-done.4
  28.5 0.0 collective-permute-done.5
  28.5 0.0 copy-done
  28.5 1.7 fusion.12
  30.2 0.0 copy-done.4
  30.2 0.1 broadcast_maximum_fusion
  30.3 0.7 fusion.10
  31.0 0.1 fusion.48
  31.1 0.0 collective-permute-done
  31.1 0.0 collective-permute-done.1
  31.1 1.1 fusion.29
  32.2 2.0 %convolution_convert_fusion = bf16[512,2048]{1,0:T(8,128)(2,1)S(1)} fusion(bf16[512,256]{0,1:T(8,128)(2,1)S(1)} %bitcast.81, bf16[1024,2048]{1,0:T(8,128)(2,1)} %param.18, s32[]{:T(128)S(6)} %select_n.9), kind=kOutput, calls=%fused_computation.9 | convolution fusion | flops 537919488 | bytes 3407876 | tf_op jit(solution)/shard_map/dot_general | solution.py:124
  34.1 0.0 copy-start.1
  34.2 30.9 %all_to_all.15 = bf16[4,128,2048]{2,1,0:T(8,128)(2,1)S(1)} all-to-all(bf16[4,128,2048]{2,1,0:T(8,128)(2,1)S(1)} %bitcast.77), channel_id=1, replica_groups=mesh['sp'=32,'tp'=4] {'tp'}, dimensions={0} | all-to-all | bytes 4194304 | tf_op jit(solution)/shard_map/all_to_all | solution.py:27
  65.0 0.0 copy-start.2
  65.0 0.4 convert_reduce_fusion.1
  65.4 0.0 copy-done.1
  65.4 0.2 fusion.32
  65.7 0.3 multiply_reduce_fusion.1
  66.0 0.0 copy-done.2
  66.0 0.3 multiply_convert_fusion.1
  66.2 0.2 broadcast_in_dim.47
  66.5 30.2 %all_to_all.16 = bf16[4,128,2048]{2,1,0:T(8,128)(2,1)S(1)} all-to-all(bf16[4,128,2048]{2,1,0:T(8,128)(2,1)S(1)} %broadcast_in_dim.47), channel_id=1, replica_groups=mesh['sp'=32,'tp'=4] {'tp'}, dimensions={0} | all-to-all | bytes 4194304 | tf_op jit(solution)/shard_map/all_to_all | solution.py:39
  96.7 0.0 all-gather.3.cloned.1.call-done
  96.7 7.6 %fusion.2 = f32[512,1408]{1,0:T(8,128)} fusion(bf16[512,2048]{1,0:T(8,128)(2,1)S(1)} %bitcast.78, bf16[2048,2816]{1,0:T(8,128)(2,1)} %all-gather.3.cloned.1.call-done), kind=kOutput, calls=%fused_computation.2 | convolution fusion | flops 2952790016 | bytes 10747904 | tf_op jit(solution)/shard_map/dot_general | solution.py:132
  104.3 18.4 %all-gather.5.cloned.1.call-done = bf16[1408,2048]{0,1:T(8,128)(2,1)} async-done(((bf16[1408,64]{0,1:T(8,128)(2,1)}), bf16[1408,2048]{0,1:T(8,128)(2,1)}) %all-gather.5.cloned.1.call-update) | async-done | bytes 5767184 | tf_op jit(solution)/shard_map/all_gather | solution.py:136
  122.7 13.3 %convolution_convert_fusion.1 = bf16[512,2048]{1,0:T(8,128)(2,1)} fusion(bf16[1408,2048]{0,1:T(8,128)(2,1)} %all-gather.5.cloned.1.call-done, bf16[512,2048]{1,0:T(8,128)(2,1)S(1)} %bitcast.79, bf16[2048,2816]{1,0:T(8,128)(2,1)} %all-gather.3.cloned.1.call-done, f32[512,1408]{1,0:T(8,128)} %fusion.2), kind=kOutput, calls=%fused_computation.11 | convolution fusion | flops 5910953984 | bytes 18612224 | tf_op jit(solution)/shard_map/dot_general | solution.py:135
  136.0 31.0 %all_to_all.17 = bf16[4,128,2048]{2,1,0:T(8,128)(2,1)S(1)} all-to-all(bf16[4,128,2048]{2,1,0:T(8,128)(2,1)} %bitcast.80), channel_id=1, replica_groups=mesh['sp'=32,'tp'=4] {'tp'}, dimensions={0} | all-to-all | bytes 4194304 | tf_op jit(solution)/shard_map/all_to_all | solution.py:27
  167.0 0.0 copy-start.3
  167.0 0.4 convert_reduce_fusion
  167.4 0.2 fusion.33
  167.6 0.3 multiply_reduce_fusion
  168.0 0.0 copy-done.3
  168.0 1.1 multiply_convert_fusion
  (8 shorter events, 0.1 us)
Async XLA Ops:
  6.5 22.0 %copy-start = (bf16[512,256]{1,0:T(8,128)(2,1)S(1)}, bf16[512,256]{1,0:T(8,128)(2,1)}, u32[]{:S(2)}) copy-start(bf16[512,256]{1,0:T(8,128)(2,1)} %param.12) | copy-start | bytes 786436
  6.5 90.2 %all-gather.3.cloned.1.call-start = ((), (), s32[]{:S(2)}) async-start(), calls=%async_computation.3 | async-start | bytes 11894784 | tf_op jit(solution)/shard_map/all_gather | solution.py:52
  8.4 21.8 %copy-start.4 = (f32[2]{0:T(128)S(1)}, f32[2]{0:T(128)}, u32[]{:S(2)}) copy-start(f32[2]{0:T(128)} %param.16) | copy-start | bytes 28
  8.4 114.4 %all-gather.5.cloned.1.call-start = ((), (), s32[]{:S(2)}) async-start(), calls=%async_computation.4 | async-start | bytes 5947392 | tf_op jit(solution)/shard_map/all_gather | solution.py:136
  9.9 15.0 %collective-permute-start.2 = (s32[128]{0:T(128)S(1)}, s32[128]{0:T(128)S(1)}, u32[]{:S(2)}, u32[]{:S(2)}) collective-permute-start(s32[128]{0:T(128)S(1)} %get-tuple-element.25), channel_id=1, source_target_pairs={{0,4},{4,8},{8,12},{12,16},{16,20},{20,24},{24,28},{28,32},{32,36}... | collective-permute-start | bytes 1544 | tf_op jit(solution)/shard_map/ppermute | solution.py:17
  11.2 15.0 %collective-permute-start.3 = (s32[128]{0:T(128)S(1)}, s32[128]{0:T(128)S(1)}, u32[]{:S(2)}, u32[]{:S(2)}) collective-permute-start(s32[128]{0:T(128)S(1)} %get-tuple-element.26), channel_id=1, source_target_pairs={{4,0},{8,4},{12,8},{16,12},{20,16},{24,20},{28,24},{32,28},{36,32}... | collective-permute-start | bytes 1544 | tf_op jit(solution)/shard_map/ppermute | solution.py:17
  13.3 15.2 %collective-permute-start.4 = (bf16[128,128]{1,0:T(8,128)(2,1)S(1)}, bf16[128,128]{1,0:T(8,128)(2,1)S(1)}, u32[]{:S(2)}, u32[]{:S(2)}) collective-permute-start(bf16[128,128]{1,0:T(8,128)(2,1)S(1)} %get-tuple-element.23), channel_id=1, source_target_pairs={{0,4},{4,8},{8,12},{12,16},{16,20},{20,24},{24,28},{28,32},{32,36}... | collective-permute-start | bytes 98312 | tf_op jit(solution)/shard_map/ppermute | solution.py:17
  18.2 10.3 %collective-permute-start.5 = (bf16[128,128]{1,0:T(8,128)(2,1)S(1)}, bf16[128,128]{1,0:T(8,128)(2,1)S(1)}, u32[]{:S(2)}, u32[]{:S(2)}) collective-permute-start(bf16[128,128]{1,0:T(8,128)(2,1)S(1)} %get-tuple-element.24), channel_id=1, source_target_pairs={{4,0},{8,4},{12,8},{16,12},{20,16},{24,20},{28,24},{32,28},{36,32}... | collective-permute-start | bytes 98312 | tf_op jit(solution)/shard_map/ppermute | solution.py:17
  20.5 10.5 %collective-permute-start = (bf16[128,128]{0,1:T(8,128)(2,1)S(1)}, bf16[128,128]{0,1:T(8,128)(2,1)S(1)}, u32[]{:S(2)}, u32[]{:S(2)}) collective-permute-start(bf16[128,128]{0,1:T(8,128)(2,1)S(1)} %get-tuple-element.21), channel_id=1, source_target_pairs={{0,4},{4,8},{8,12},{12,16},{16,20},{20,24},{24,28},{28,32},{32,36}... | collective-permute-start | bytes 98312 | tf_op jit(solution)/shard_map/ppermute | solution.py:17
  24.9 6.2 %collective-permute-start.1 = (bf16[128,128]{0,1:T(8,128)(2,1)S(1)}, bf16[128,128]{0,1:T(8,128)(2,1)S(1)}, u32[]{:S(2)}, u32[]{:S(2)}) collective-permute-start(bf16[128,128]{0,1:T(8,128)(2,1)S(1)} %get-tuple-element.22), channel_id=1, source_target_pairs={{4,0},{8,4},{12,8},{16,12},{20,16},{24,20},{28,24},{32,28},{36,32}... | collective-permute-start | bytes 98312 | tf_op jit(solution)/shard_map/ppermute | solution.py:17
  34.1 31.3 %copy-start.1 = (bf16[128,2048]{1,0:T(8,128)(2,1)S(1)}, bf16[128,2048]{1,0:T(8,128)(2,1)}, u32[]{:S(2)}) copy-start(bf16[128,2048]{1,0:T(8,128)(2,1)} %param.17) | copy-start | bytes 1572868
  65.0 0.9 copy-start.2
  167.0 1.0 copy-start.3
Sparse Core Ops, SparseCore 0:
  9.6 63.0 all-gather.2
  75.0 47.7 all-gather.4
where the time goes:
time: 177 us; the launch traced here: 176 us
  blocking collectives  92.1 us (52%)
  matrix products  25.6 us (14%)
  waiting for transfers between devices  19.1 us (11%)
  starting transfers between devices  14.4 us (8%)
  between operations  13.6 us (8%)
  other arithmetic  8.19 us (5%)
  local copies, waits for them, and re-layouts  2.83 us (2%)
    all_to_all x2, blocking collectives, sum_at_owner(): lax.all_to_all(split_up(value, dim, devices), axis, 0, 0, tiled=True)  61.9 us
    all_to_all x1, blocking collectives, sent_to_all(): return lax.all_to_all(copies, axis, split_axis=0, concat_axis=0, tiled=True)  30.2 us
    all_gather x1, waiting for transfers between devices, per_device(): lax.all_gather(w_down, 'sp', axis=1, tiled=True)  18.4 us
    ppermute x6, starting transfers between devices, shifted(): lax.ppermute(value, axis, [(source, source + steps) for source in range(l...  14.4 us
    dot_general x1, matrix products, per_device(): jnp.dot(hidden, lax.all_gather(w_down, 'sp', axis=1, tiled=True), preferr...  13.3 us
    dot_general x1, matrix products, per_device(): jnp.dot(whole_rows, gate_whole, preferred_element_type=jnp.float32)  7.62 us
  transfers between devices with their start and end apart: 8, of which 1 were waited for; matrix products, arithmetic and copies ran while one was open for 11% of the time, Pallas kernels for 0%

commit v1 on v0

--- a/solution.py
+++ b/solution.py
@@ -133,7 +133,9 @@
     up_part = jnp.dot(whole_rows, up_whole, preferred_element_type=jnp.float32)
     hidden = (jax.nn.silu(gate_part) * up_part).astype(jnp.bfloat16)
     down_terms = jnp.dot(
-        hidden, lax.all_gather(w_down, "sp", axis=1, tiled=True), preferred_element_type=jnp.float32
+        hidden,
+        jnp.concatenate(lax.all_gather(w_down, "sp"), axis=1),
+        preferred_element_type=jnp.float32,
     )
     rounded = lax.optimization_barrier(down_terms.astype(jnp.bfloat16)).astype(jnp.float32)
     down_rows = sum_at_owner(rounded.astype(jnp.bfloat16), "tp", 0)

time: 177 us -> 184 us (1.040)
  blocking collectives: 92.1 us -> 61.9 us
  waiting for transfers between devices: 19.1 us -> 43.2 us
  local copies, waits for them, and re-layouts: 2.83 us -> 12.3 us
  starting transfers between devices: 14.4 us -> 18.2 us
    all_to_all x1 -> x0, blocking collectives: 30.2 us -> none  [sent_to_all(): return lax.all_to_all(copies, axis, split_axis=0, concat_axis=0, tiled=True)]
    all_gather x1, waiting for transfers between devices: 0.01 us -> 23.1 us  [in_one_piece(): lax.all_gather(both, axis, axis=dim, tiled=True)]
    all_to_all x0 -> x1, waiting for transfers between devices: none -> 19.3 us  [sent_to_all(): return lax.all_to_all(copies, axis, split_axis=0, concat_axis=0, tiled=True)]
    all_gather x1, waiting for transfers between devices: 18.4 us -> 0.02 us  [per_device(): lax.all_gather(w_down, 'sp')]
    reshape x0 -> x1, local copies, waits for them, and re-layouts: none -> 4.43 us  [per_device(): jnp.concatenate(lax.all_gather(w_down, 'sp'), axis=1)]
    all_to_all x0 -> x1, starting transfers between devices: none -> 3.79 us  [sent_to_all(): return lax.all_to_all(copies, axis, split_axis=0, concat_axis=0, tiled=True)]
    unnamed x11 -> x12, local copies, waits for them, and re-layouts: 1.03 us -> 4.72 us
  transfers between devices with their start and end apart: 8 -> 9, of which waited for: 1 -> 2; matrix products, arithmetic and copies ran while one was open for 11% -> 13% of each run, Pallas kernels for 0% -> 0%
where the time goes in v1:
time: 184 us; the launch traced here: 183 us
  blocking collectives  61.9 us (34%)
  waiting for transfers between devices  43.2 us (23%)
  matrix products  25.6 us (14%)
  starting transfers between devices  18.2 us (10%)
  between operations  13.7 us (7%)
  local copies, waits for them, and re-layouts  12.3 us (7%)
  other arithmetic  8.15 us (4%)
    all_to_all x2, blocking collectives, sum_at_owner(): lax.all_to_all(split_up(value, dim, devices), axis, 0, 0, tiled=True)  61.9 us
    all_gather x1, waiting for transfers between devices, in_one_piece(): lax.all_gather(both, axis, axis=dim, tiled=True)  23.1 us
    all_to_all x1, waiting for transfers between devices, sent_to_all(): return lax.all_to_all(copies, axis, split_axis=0, concat_axis=0, tiled=True)  19.3 us
    ppermute x6, starting transfers between devices, shifted(): lax.ppermute(value, axis, [(source, source + steps) for source in range(l...  14.4 us
    dot_general x1, matrix products, per_device(): jnp.dot(hidden, jnp.concatenate(lax.all_gather(w_down, 'sp'), axis=1), pr...  13.2 us
    dot_general x1, matrix products, per_device(): jnp.dot(whole_rows, gate_whole, preferred_element_type=jnp.float32)  7.62 us
    unnamed x12, local copies, waits for them, and re-layouts  4.72 us
    reshape x1, local copies, waits for them, and re-layouts, per_device(): jnp.concatenate(lax.all_gather(w_down, 'sp'), axis=1)  4.43 us
  transfers between devices with their start and end apart: 9, of which 2 were waited for; matrix products, arithmetic and copies ran while one was open for 13% of the time, Pallas kernels for 0%

profile of v1, /device:TPU:0, one launch (start us, length us, event | category | flops | bytes accessed | tf_op | source)
XLA Modules:
  0.0 183.0 jit_solution(11322674819101030510)
XLA Ops:
  6.5 0.0 copy-start
  6.5 0.0 all-gather.6.cloned.1.call-start
  6.5 0.7 all-gather.6.cloned.1.call-update
  7.3 0.0 copy-start.4
  7.3 0.0 all-gather.4.cloned.1.call-start
  7.3 1.8 pad_maximum_fusion
  9.1 0.0 all-gather.4.cloned.1.call-update
  9.1 0.8 fusion.59
  9.9 1.3 collective-permute-start.2
  11.2 1.3 collective-permute-start.3
  12.5 0.8 fusion.58
  13.2 4.9 %collective-permute-start.4 = (bf16[128,128]{1,0:T(8,128)(2,1)S(1)}, bf16[128,128]{1,0:T(8,128)(2,1)S(1)}, u32[]{:S(2)}, u32[]{:S(2)}) collective-permute-start(bf16[128,128]{1,0:T(8,128)(2,1)S(1)} %get-tuple-element.23), channel_id=1, source_target_pairs={{0,4},{4,8},{8,12},{12,16},{16,20},{20,24},{24,28},{28,32},{32,36}... | collective-permute-start | bytes 98312 | tf_op jit(solution)/shard_map/ppermute | solution.py:17
  18.2 1.3 collective-permute-start.5
  19.5 1.0 copy.23
  20.5 4.3 %collective-permute-start = (bf16[128,128]{0,1:T(8,128)(2,1)S(1)}, bf16[128,128]{0,1:T(8,128)(2,1)S(1)}, u32[]{:S(2)}, u32[]{:S(2)}) collective-permute-start(bf16[128,128]{0,1:T(8,128)(2,1)S(1)} %get-tuple-element.21), channel_id=1, source_target_pairs={{0,4},{4,8},{8,12},{12,16},{16,20},{20,24},{24,28},{28,32},{32,36}... | collective-permute-start | bytes 98312 | tf_op jit(solution)/shard_map/ppermute | solution.py:17
  24.9 0.0 collective-permute-done.2
  24.9 1.3 collective-permute-start.1
  26.2 0.0 collective-permute-done.3
  26.2 0.7 pad_add_fusion
  26.9 1.6 fusion.18
  28.5 0.0 collective-permute-done.4
  28.5 0.0 collective-permute-done.5
  28.5 0.0 copy-done
  28.5 1.7 fusion.12
  30.2 0.0 copy-done.4
  30.2 0.1 broadcast_maximum_fusion
  30.2 0.7 fusion.10
  31.0 0.1 fusion.48
  31.0 0.0 collective-permute-done
  31.1 0.0 collective-permute-done.1
  31.1 1.1 fusion.29
  32.2 2.0 %convolution_convert_fusion = bf16[512,2048]{1,0:T(8,128)(2,1)S(1)} fusion(bf16[512,256]{0,1:T(8,128)(2,1)S(1)} %bitcast.91, bf16[1024,2048]{1,0:T(8,128)(2,1)} %param.18, s32[]{:T(128)S(6)} %select_n.9), kind=kOutput, calls=%fused_computation.9 | convolution fusion | flops 537919488 | bytes 3407876 | tf_op jit(solution)/shard_map/dot_general | solution.py:124
  34.2 0.0 copy-start.1
  34.2 30.9 %all_to_all.15 = bf16[4,128,2048]{2,1,0:T(8,128)(2,1)S(1)} all-to-all(bf16[4,128,2048]{2,1,0:T(8,128)(2,1)S(1)} %bitcast.85), channel_id=1, replica_groups=mesh['sp'=32,'tp'=4] {'tp'}, dimensions={0} | all-to-all | bytes 4194304 | tf_op jit(solution)/shard_map/all_to_all | solution.py:27
  65.1 0.0 copy-start.2
  65.1 0.4 convert_reduce_fusion.1
  65.5 0.0 copy-done.1
  65.5 0.2 fusion.32
  65.7 0.3 multiply_reduce_fusion.1
  66.0 0.0 copy-done.2
  66.0 0.3 multiply_convert_fusion.1
  66.3 1.6 broadcast_in_dim.47
  67.9 3.8 %all-to-all-start.1 = ((bf16[4,128,2048]{2,1,0:T(8,128)(2,1)}), bf16[4,128,2048]{2,1,0:T(8,128)(2,1)S(1)}, u32[]{:S(2)}, u32[]{:S(2)}) async-start(bf16[4,128,2048]{2,1,0:T(8,128)(2,1)} %broadcast_in_dim.47), calls=%async_computation.1 | async-start | bytes 4194304 | tf_op jit(solution)/shard_map/all_to_all | solution.py:39
  71.7 0.0 all-gather.6.cloned.1.call-done
  71.7 3.7 %copy.31 = bf16[8,8,32,1408]{3,2,1,0:T(8,128)(2,1)S(1)} copy(bf16[8,8,32,1408]{3,1,2,0:T(8,128)(2,1)} %bitcast.86) | data formatting | bytes 11534336
  75.4 4.4 %copy.28 = bf16[1408,32,64]{0,2,1:T(8,128)(2,1)} copy(bf16[1408,32,64]{0,1,2:T(8,128)(2,1)S(1)} %bitcast.84) | data formatting | bytes 11534336 | tf_op jit(solution)/shard_map/reshape | solution.py:137
  79.9 19.3 %all-to-all-done.1 = bf16[4,128,2048]{2,1,0:T(8,128)(2,1)S(1)} async-done(((bf16[4,128,2048]{2,1,0:T(8,128)(2,1)}), bf16[4,128,2048]{2,1,0:T(8,128)(2,1)S(1)}, u32[]{:S(2)}, u32[]{:S(2)}) %all-to-all-start.1) | async-done | bytes 2097184 | tf_op jit(solution)/shard_map/all_to_all | solution.py:39
  99.2 23.1 %all-gather.4.cloned.1.call-done = bf16[2048,2816]{1,0:T(8,128)(2,1)} async-done(((bf16[64,2816]{1,0:T(8,128)(2,1)}), bf16[2048,2816]{1,0:T(8,128)(2,1)}) %all-gather.4.cloned.1.call-update) | async-done | bytes 11534352 | tf_op jit(solution)/shard_map/all_gather | solution.py:52
  122.3 7.6 %fusion.2 = f32[512,1408]{1,0:T(8,128)} fusion(bf16[512,2048]{1,0:T(8,128)(2,1)S(1)} %bitcast.88, bf16[2048,2816]{1,0:T(8,128)(2,1)} %all-gather.4.cloned.1.call-done), kind=kOutput, calls=%fused_computation.2 | convolution fusion | flops 2952790016 | bytes 10747904 | tf_op jit(solution)/shard_map/dot_general | solution.py:132
  129.9 13.2 %convolution_convert_fusion.1 = bf16[512,2048]{1,0:T(8,128)(2,1)} fusion(bf16[1408,2048]{0,1:T(8,128)(2,1)} %bitcast.87, bf16[512,2048]{1,0:T(8,128)(2,1)S(1)} %bitcast.89, bf16[2048,2816]{1,0:T(8,128)(2,1)} %all-gather.4.cloned.1.call-done, f32[512,1408]{1,0:T(8,128)} %fusion.2), kind=kOutput, calls=%fused_computation.11 | convolution fusion | flops 5910953984 | bytes 18612224 | tf_op jit(solution)/shard_map/dot_general | solution.py:135
  143.1 31.0 %all_to_all.16 = bf16[4,128,2048]{2,1,0:T(8,128)(2,1)S(1)} all-to-all(bf16[4,128,2048]{2,1,0:T(8,128)(2,1)} %bitcast.90), channel_id=1, replica_groups=mesh['sp'=32,'tp'=4] {'tp'}, dimensions={0} | all-to-all | bytes 4194304 | tf_op jit(solution)/shard_map/all_to_all | solution.py:27
  174.1 0.0 copy-start.3
  174.1 0.4 convert_reduce_fusion
  174.5 0.2 fusion.33
  174.8 0.3 multiply_reduce_fusion
  175.1 0.0 copy-done.3
  175.1 1.1 multiply_convert_fusion
  (8 shorter events, 0.1 us)
Async XLA Ops:
  6.5 22.0 %copy-start = (bf16[512,256]{1,0:T(8,128)(2,1)S(1)}, bf16[512,256]{1,0:T(8,128)(2,1)}, u32[]{:S(2)}) copy-start(bf16[512,256]{1,0:T(8,128)(2,1)} %param.12) | copy-start | bytes 786436
  6.5 65.2 %all-gather.6.cloned.1.call-start = ((), (), s32[]{:S(2)}) async-start(), calls=%async_computation.4 | async-start | bytes 5947392 | tf_op jit(solution)/shard_map/all_gather | solution.py:137
  7.3 22.9 %copy-start.4 = (f32[2]{0:T(128)S(1)}, f32[2]{0:T(128)}, u32[]{:S(2)}) copy-start(f32[2]{0:T(128)} %param.16) | copy-start | bytes 28
  7.3 115.0 %all-gather.4.cloned.1.call-start = ((), (), s32[]{:S(2)}) async-start(), calls=%async_computation.3 | async-start | bytes 11894784 | tf_op jit(solution)/shard_map/all_gather | solution.py:52
  9.9 15.0 %collective-permute-start.2 = (s32[128]{0:T(128)S(1)}, s32[128]{0:T(128)S(1)}, u32[]{:S(2)}, u32[]{:S(2)}) collective-permute-start(s32[128]{0:T(128)S(1)} %get-tuple-element.25), channel_id=1, source_target_pairs={{0,4},{4,8},{8,12},{12,16},{16,20},{20,24},{24,28},{28,32},{32,36}... | collective-permute-start | bytes 1544 | tf_op jit(solution)/shard_map/ppermute | solution.py:17
  11.2 15.0 %collective-permute-start.3 = (s32[128]{0:T(128)S(1)}, s32[128]{0:T(128)S(1)}, u32[]{:S(2)}, u32[]{:S(2)}) collective-permute-start(s32[128]{0:T(128)S(1)} %get-tuple-element.26), channel_id=1, source_target_pairs={{4,0},{8,4},{12,8},{16,12},{20,16},{24,20},{28,24},{32,28},{36,32}... | collective-permute-start | bytes 1544 | tf_op jit(solution)/shard_map/ppermute | solution.py:17
  13.2 15.2 %collective-permute-start.4 = (bf16[128,128]{1,0:T(8,128)(2,1)S(1)}, bf16[128,128]{1,0:T(8,128)(2,1)S(1)}, u32[]{:S(2)}, u32[]{:S(2)}) collective-permute-start(bf16[128,128]{1,0:T(8,128)(2,1)S(1)} %get-tuple-element.23), channel_id=1, source_target_pairs={{0,4},{4,8},{8,12},{12,16},{16,20},{20,24},{24,28},{28,32},{32,36}... | collective-permute-start | bytes 98312 | tf_op jit(solution)/shard_map/ppermute | solution.py:17
  18.2 10.3 %collective-permute-start.5 = (bf16[128,128]{1,0:T(8,128)(2,1)S(1)}, bf16[128,128]{1,0:T(8,128)(2,1)S(1)}, u32[]{:S(2)}, u32[]{:S(2)}) collective-permute-start(bf16[128,128]{1,0:T(8,128)(2,1)S(1)} %get-tuple-element.24), channel_id=1, source_target_pairs={{4,0},{8,4},{12,8},{16,12},{20,16},{24,20},{28,24},{32,28},{36,32}... | collective-permute-start | bytes 98312 | tf_op jit(solution)/shard_map/ppermute | solution.py:17
  20.5 10.5 %collective-permute-start = (bf16[128,128]{0,1:T(8,128)(2,1)S(1)}, bf16[128,128]{0,1:T(8,128)(2,1)S(1)}, u32[]{:S(2)}, u32[]{:S(2)}) collective-permute-start(bf16[128,128]{0,1:T(8,128)(2,1)S(1)} %get-tuple-element.21), channel_id=1, source_target_pairs={{0,4},{4,8},{8,12},{12,16},{16,20},{20,24},{24,28},{28,32},{32,36}... | collective-permute-start | bytes 98312 | tf_op jit(solution)/shard_map/ppermute | solution.py:17
  24.9 6.2 %collective-permute-start.1 = (bf16[128,128]{0,1:T(8,128)(2,1)S(1)}, bf16[128,128]{0,1:T(8,128)(2,1)S(1)}, u32[]{:S(2)}, u32[]{:S(2)}) collective-permute-start(bf16[128,128]{0,1:T(8,128)(2,1)S(1)} %get-tuple-element.22), channel_id=1, source_target_pairs={{4,0},{8,4},{12,8},{16,12},{20,16},{24,20},{28,24},{32,28},{36,32}... | collective-permute-start | bytes 98312 | tf_op jit(solution)/shard_map/ppermute | solution.py:17
  34.2 31.3 %copy-start.1 = (bf16[128,2048]{1,0:T(8,128)(2,1)S(1)}, bf16[128,2048]{1,0:T(8,128)(2,1)}, u32[]{:S(2)}) copy-start(bf16[128,2048]{1,0:T(8,128)(2,1)} %param.17) | copy-start | bytes 1572868
  65.1 0.9 copy-start.2
  67.9 31.3 %all-to-all-start.1 = ((bf16[4,128,2048]{2,1,0:T(8,128)(2,1)}), bf16[4,128,2048]{2,1,0:T(8,128)(2,1)S(1)}, u32[]{:S(2)}, u32[]{:S(2)}) async-start(bf16[4,128,2048]{2,1,0:T(8,128)(2,1)} %broadcast_in_dim.47), calls=%async_computation.1 | async-start | bytes 4194304 | tf_op jit(solution)/shard_map/all_to_all | solution.py:39
  174.1 1.0 copy-start.3
Sparse Core Ops, SparseCore 0:
  9.7 50.9 all-gather.5
  63.0 59.2 all-gather.3
